TPU v7x, 32 devices: a whole 2x2x4 slice. The times are simulated.
32 devices in a mesh: sp: 8 (over z, x), tp: 4 (over y, core).
Axes of the slice: x: 2, y: 2, z: 4, core: 2. Of those that a mesh axis runs over, the one named last changes fastest.
Arguments:
- tokens: bfloat16 [4096, 4096], P('sp', 'tp'), may hold values from -8 to 8
- w_key: bfloat16 [4096, 2048], P(None, 'tp'), may hold values from -0.09375 to 0.09375
- w_value: bfloat16 [4096, 2048], P(None, 'tp'), may hold values from -0.09375 to 0.09375
- w_beta: bfloat16 [4096, 16], replicated, may hold values from -0.09375 to 0.09375
- w_decay: bfloat16 [4096, 16], replicated, may hold values from -0.09375 to 0.09375
- beta_bias: float32 [16], replicated, may hold values from -6 to -4
- decay_rate: float32 [16], replicated, as said below
- forgetting_increment: float32 [16, 4096], P('tp', 'sp')
- new_query: bfloat16 [16, 128], P('tp', 'sp'), may hold values from -6 to 6
- read_gain: bfloat16 [128], replicated, may hold values from 0.099609375 to 1.8984375
Outputs:
- state_cache: bfloat16 [16, 128, 128], P('tp', 'sp')
- first_read: float32 [16, 128], P('tp')
Inputs may be any that keep to these rules, and one draw needn't show every extreme that they name: `decay_rate`: positive.
All inputs are finite; a program needn't handle non-finite values.
Results may differ from a plain program's by a relative error of at most 0.0075.
Values may be sent and summed in bfloat16 or wider, within the bound.
A program may use at most 64 MiB of HBM per device.

v0:
```python
import jax
import jax.numpy as jnp
from jax import lax
from jax.sharding import PartitionSpec as P

DK = 128
DV = 128
BLOCK = 64


norm_eps = 1e-06


def prefix(part, axis, combine, identity):
    count = lax.axis_size(axis)
    place = lax.axis_index(axis)
    ahead = count - 1 - place
    gathered = lax.all_gather(part, axis)
    state = jnp.zeros_like(part) + jnp.asarray(identity, part.dtype)

    def one(lap, state):
        source = count - 1 - lap
        return combine(state, lax.dynamic_index_in_dim(gathered, source, 0, False))

    return lax.fori_loop(0, ahead, one, state)


def matmul_f32(left, right):
    return jnp.dot(left, right, precision=lax.Precision.HIGHEST)


def batched_f32(left, right):
    return jnp.einsum("hij,hjk->hik", left, right, precision=lax.Precision.HIGHEST)


def unit_inverse(lower):
    current_size = lower.shape[0]
    identity = jnp.eye(current_size, dtype=jnp.float32)
    result = identity - lower
    lower_power = lower
    covered = 2
    while covered < current_size:
        lower_power = matmul_f32(lower_power, lower_power)
        result = matmul_f32(result, identity + lower_power)
        covered = covered * 2
    return result


def block_terms(key_blk, value_blk, beta_blk, logd_blk):
    current_size = key_blk.shape[0]
    cumulative = jnp.cumsum(logd_blk)
    spread = cumulative[:, None] - cumulative[None, :]
    location_positions = jnp.arange(current_size)
    causal = location_positions[:, None] >= location_positions[None, :]
    strict = location_positions[:, None] > location_positions[None, :]
    decay_table = jnp.where(causal, jnp.exp(jnp.where(causal, spread, 0.0)), 0.0)
    key_beta = key_blk * beta_blk[:, None]
    lower = jnp.where(strict, matmul_f32(key_beta, key_blk.T) * decay_table, 0.0)
    inverse = unit_inverse(lower)
    update = matmul_f32(inverse, value_blk * beta_blk[:, None])
    erase = matmul_f32(inverse, key_beta * jnp.exp(cumulative)[:, None])
    key_remainder = key_blk * jnp.exp(cumulative[-1] - cumulative)[:, None]
    return (update, erase, key_remainder, jnp.exp(cumulative[-1]))


def per_device(
    tokens,
    w_key,
    w_value,
    w_beta,
    w_decay,
    beta_bias,
    decay_rate,
    forgetting_increment,
    new_query,
    read_gain,
):
    heads_here = w_key.shape[1] // DK
    token_count = tokens.shape[0]
    head_start = lax.axis_index("tp") * heads_here
    gate_weights = jnp.concatenate(
        [
            lax.dynamic_slice_in_dim(w_beta, head_start, heads_here, 1),
            lax.dynamic_slice_in_dim(w_decay, head_start, heads_here, 1),
        ],
        axis=1,
    )
    piece = lax.all_gather(tokens, "tp", axis=1, tiled=True)
    key_acc = jnp.dot(piece, w_key, preferred_element_type=jnp.float32)
    value_acc = jnp.dot(piece, w_value, preferred_element_type=jnp.float32)
    gate_acc = jnp.dot(piece, gate_weights, preferred_element_type=jnp.float32)
    key_wide = (
        lax.optimization_barrier(key_acc.astype(jnp.bfloat16))
        .astype(jnp.float32)
        .reshape(token_count, heads_here, DK)
    )
    key_unit = key_wide * lax.rsqrt(jnp.sum(key_wide * key_wide, axis=-1, keepdims=True) + norm_eps)
    value_wide = (
        lax.optimization_barrier(value_acc.astype(jnp.bfloat16))
        .astype(jnp.float32)
        .reshape(token_count, heads_here, DV)
    )
    bias_here = lax.dynamic_slice_in_dim(beta_bias, head_start, heads_here, 0)
    rate_here = lax.dynamic_slice_in_dim(decay_rate, head_start, heads_here, 0)
    beta = jax.nn.sigmoid(gate_acc[:, :heads_here] + bias_here).T
    log_decay = (
        -rate_here[:, None] * jax.nn.softplus(gate_acc[:, heads_here:].T) + forgetting_increment
    )
    blocks = token_count // BLOCK
    key_heads = key_unit.transpose(1, 0, 2).reshape(heads_here, blocks, BLOCK, DK)
    value_heads = value_wide.transpose(1, 0, 2).reshape(heads_here, blocks, BLOCK, DV)
    terms = jax.vmap(jax.vmap(block_terms))(
        key_heads,
        value_heads,
        beta.reshape(heads_here, blocks, BLOCK),
        log_decay.reshape(heads_here, blocks, BLOCK),
    )
    inputs = tuple((jnp.moveaxis(item, 1, 0) for item in terms))
    identity = jnp.broadcast_to(jnp.eye(DK, dtype=jnp.float32), (heads_here, DK, DK))
    value_zeros = jnp.zeros((heads_here, DK, DV), jnp.float32)
    padding = jnp.zeros((heads_here, BLOCK, DK), jnp.float32)

    def advance(state, block_in):
        update, erase, key_remainder, keep = block_in
        fresh = jnp.concatenate([update, padding], axis=-1) - jnp.einsum(
            "hcd,hde->hce", erase, state, precision=lax.Precision.HIGHEST
        )
        state = keep[:, None, None] * state + jnp.einsum(
            "hcd,hce->hde", key_remainder, fresh, precision=lax.Precision.HIGHEST
        )
        return (state, None)

    combined, _ = lax.scan(advance, jnp.concatenate([value_zeros, identity], axis=-1), inputs)
    local_b = combined[:, :, :DV]
    local_left = combined[:, :, DV:]
    later_product = prefix(local_left, "sp", batched_f32, identity)
    summed = lax.psum_scatter(
        batched_f32(later_product, local_b), "sp", scatter_dimension=1, tiled=True
    )
    own_rows = summed.astype(jnp.bfloat16)
    partial_read = jnp.sum(
        new_query.astype(jnp.float32)[:, :, None] * own_rows.astype(jnp.float32), axis=1
    )
    raw_read = lax.psum(partial_read, "sp")
    first_read = (
        raw_read
        * lax.rsqrt(jnp.mean(raw_read * raw_read, axis=-1, keepdims=True) + norm_eps)
        * read_gain.astype(jnp.float32)
    )
    return (own_rows, first_read)


def solution(mesh):
    return jax.shard_map(
        per_device,
        mesh=mesh,
        in_specs=(
            P("sp", "tp"),
            P(None, "tp"),
            P(None, "tp"),
            P(),
            P(),
            P(),
            P(),
            P("tp", "sp"),
            P("tp", "sp"),
            P(),
        ),
        out_specs=(P("tp", "sp", None), P("tp", None)),
        check_vma=False,
    )
```

profile of v0, /device:TPU:0, one launch (start us, length us, event | category | flops | bytes accessed | tf_op | source)
XLA Modules:
  0.0 263.8 jit_solution(13869263426340788410)
XLA Ops:
  11.1 35.6 %all-gather.4.cloned.1.call-done = bf16[512,4096]{1,0:T(8,128)(2,1)} async-done(((bf16[512,1024]{1,0:T(8,128)(2,1)}), bf16[512,4096]{1,0:T(8,128)(2,1)}) %all-gather.4.cloned.1.call-update) | async-done | bytes 4194320 | tf_op jit(solution)/shard_map/all_gather | solution.py:88
  46.8 3.4 %convolution_bitcast_fusion.3 = f32[512,8]{0,1:T(8,128)S(1)} fusion(bf16[512,4096]{1,0:T(8,128)(2,1)} %all-gather.4.cloned.1.call-done, bf16[4096,4]{0,1:T(4,128)(2,1)S(1)} %get-tuple-element.148, bf16[4096,4]{0,1:T(4,128)(2,1)S(1)} %get-tuple-element.149), kind=kOutput, calls=%fused_computation.25 | convolution fusion | flops 33685504 | bytes 4276224 | tf_op jit(solution)/shard_map/dot_general | solution.py:91
  52.9 5.9 %convolution_convert_fusion.1 = bf16[512,512]{1,0:T(8,128)(2,1)S(1)} fusion(bf16[512,4096]{1,0:T(8,128)(2,1)} %all-gather.4.cloned.1.call-done, bf16[4096,512]{1,0:T(8,128)(2,1)} %param.15), kind=kOutput, calls=%fused_computation.24 | convolution fusion | flops 2147745792 | bytes 8912896 | tf_op jit(solution)/shard_map/dot_general | solution.py:89
  58.8 2.3 convolution_convert_fusion
  62.7 2.1 multiply_bitcast_fusion
  64.7 2.7 %fusion.15 = f32[4,8,64,64]{3,2,1,0:T(8,128)S(1)} fusion(f32[4,8,64,128]{3,2,1,0:T(8,128)S(1)} %bitcast.101, f32[4,8,64]{2,1,0:T(8,128)S(1)} %reduce_window_sum.11, f32[4,8,64]{2,1,0:T(8,128)S(1)} %mul.102, pred[64,64]{1,0:T(8,128)(4,1)} %get-tuple-element.150, pred[64,64]{1,0:T(8,128)(4,1)} %get-tuple-element.151), kind=kOutput, calls=%fused_computation.22 | convolution fusion | flops 202244096 | bytes 1597440 | tf_op jit(solution)/shard_map/vmap(vmap())/dot_general | solution.py:29
  72.2 1.4 fusion.23
  79.6 2.6 convolution_bitcast_fusion.1
  83.5 29.7 %while.22 = (s32[]{:T(128)}, f32[4,128,256]{2,1,0:T(8,128)S(1)}, f32[8,4]{1,0:T(8,128)}, f32[8,4,64,128]{3,2,0,1:T(8,128)}, f32[8,4,64,128]{3,2,0,1:T(8,128)S(1)}, /*index=5*/f32[8,4,64,128]{3,2,0,1:T(8,128)}, s32[]{:T(128)}) while((s32[]{:T(128)}, f32[4,128,256]{2,1,0:T(8,128)S(1)}, f32[8,4]{1,0:T(8,128)}, f32[8,4,64,128]{3,2,0,1:T(8,128)}, ...), condition=%wide.region_3.4_spmd, body=%wide.region_2.3_spmd.sunk | while | flops 201654272 | bytes 2752661 | solution.py:133
  85.5 1.7 convolution_add_fusion.3
  87.9 1.3 convolution_subtract_fusion.2
  89.2 1.7 convolution_add_fusion.3
  91.6 1.3 convolution_subtract_fusion.2
  92.9 1.7 convolution_add_fusion.3
  95.3 1.3 convolution_subtract_fusion.2
  96.7 1.7 convolution_add_fusion.3
  100.4 1.7 convolution_add_fusion.3
  104.1 1.7 convolution_add_fusion.3
  107.8 1.7 convolution_add_fusion.3
  111.5 1.7 convolution_add_fusion.3
  114.0 49.2 %all-gather.6.cloned.1.call-done = f32[32,128,128]{2,1,0:T(8,128)} async-done(((f32[4,128,128]{2,1,0:T(8,128)}), f32[32,128,128]{2,1,0:T(8,128)}) %all-gather.6.cloned.1.call-update) | async-done | bytes 2097168 | tf_op jit(solution)/shard_map/all_gather | solution.py:18
  163.2 11.3 %while.23 = (s32[]{:T(128)}, f32[4,128,128]{1,2,0:T(8,128)S(1)}, s32[]{:T(128)}, f32[8,4,128,128]{3,2,1,0:T(8,128)}, s32[]{:T(128)}, /*index=5*/s32[]{:T(128)}, s32[]{:T(128)}, s32[]{:T(128)}) while((s32[]{:T(128)}, f32[4,128,128]{1,2,0:T(8,128)S(1)}, s32[]{:T(128)}, f32[8,4,128,128]{3,2,1,0:T(8,128)}, s32[]{:T(128)}, /*index=5*/s32[]{:T(128)}, ...), condition=%wide.region_5.6_spmd, body=%wide.region_4.5_spmd.sunk | while | flops 100663304 | bytes 1310863 | solution.py:25
  163.3 1.6 convolution_bitcast_fusion.5
  164.9 1.6 convolution_bitcast_fusion.5
  166.5 1.6 convolution_bitcast_fusion.5
  168.1 1.6 convolution_bitcast_fusion.5
  169.7 1.6 convolution_bitcast_fusion.5
  171.3 1.6 convolution_bitcast_fusion.5
  172.9 1.6 convolution_bitcast_fusion.5
  175.9 59.9 %reduce-scatter.2.cloned.1.call-done = f32[4,16,128]{2,1,0:T(8,128)} async-done(((f32[4,128,128]{2,1,0:T(8,128)}), f32[4,16,128]{2,1,0:T(8,128)}) %reduce-scatter.2.cloned.1.call-update) | async-done | bytes 32784 | tf_op jit(solution)/shard_map/reduce_scatter | solution.py:137
  235.7 1.4 multiply_reduce_fusion.1
  237.1 19.4 %psum.7 = f32[4,128]{1,0:T(4,128)S(1)} all-reduce(f32[4,128]{1,0:T(4,128)S(1)} %get-tuple-element.144), channel_id=1, replica_groups=mesh['sp'=8,'tp'=4] {'sp'}, use_global_device_ids=true, to_apply=%region_8.9 | all-reduce | flops 512 | bytes 4096 | tf_op jit(solution)/shard_map/psum | solution.py:144
  (86 shorter events, 35.4 us)
Async XLA Ops:
  7.2 43.0 %copy-start.1 = (f32[4,512]{1,0:T(4,128)S(1)}, f32[4,512]{1,0:T(4,128)}, u32[]{:S(2)}) copy-start(f32[4,512]{1,0:T(4,128)} %param.21) | copy-start | bytes 24580
  7.2 39.6 %all-gather.4.cloned.1.call-start = ((), (), s32[]{:S(2)}) async-start(), calls=%async_computation.1 | async-start | bytes 5242880 | tf_op jit(solution)/shard_map/all_gather | solution.py:88
  7.9 155.3 %all-gather.6.cloned.1.call-start = ((), (), s32[]{:S(2)}) async-start(), calls=%async_computation.3 | async-start | bytes 2359296 | tf_op jit(solution)/shard_map/all_gather | solution.py:18
  52.9 5.9 %copy-start = (bf16[512,4096]{1,0:T(8,128)(2,1)S(1)}, bf16[512,4096]{1,0:T(8,128)(2,1)}, u32[]{:S(2)}) copy-start(bf16[512,4096]{1,0:T(8,128)(2,1)} %all-gather.4.cloned.1.call-done) | copy-start | bytes 12582916
  52.9 5.9 %copy-start.3 = (bf16[4096,512]{1,0:T(8,128)(2,1)S(1)}, bf16[4096,512]{1,0:T(8,128)(2,1)}, u32[]{:S(2)}) copy-start(bf16[4096,512]{1,0:T(8,128)(2,1)} %param.16) | copy-start | bytes 12582916
  113.9 61.9 %copy-start.4 = (bf16[128]{0:T(256)(128)(2,1)S(1)}, bf16[128]{0:T(256)(128)(2,1)}, u32[]{:S(2)}) copy-start(bf16[128]{0:T(256)(128)(2,1)} %param.23) | copy-start | bytes 772
  113.9 61.9 %copy-start.2 = (bf16[4,16]{1,0:T(4,128)(2,1)S(1)}, bf16[4,16]{1,0:T(4,128)(2,1)}, u32[]{:S(2)}) copy-start(bf16[4,16]{1,0:T(4,128)(2,1)} %param.22) | copy-start | bytes 388
  113.9 121.8 %reduce-scatter.2.cloned.1.call-start = ((), (), s32[]{:S(2)}) async-start(), calls=%async_computation.2 | async-start | bytes 294912 | tf_op jit(solution)/shard_map/reduce_scatter | solution.py:137
Sparse Core Ops, SparseCore 0:
  9.5 37.1 all-gather.3
  114.1 49.0 all-gather.5
  175.9 59.7 reduce-scatter.1
where the time goes:
time: 265 us; the launch traced here: 264 us
  waiting for transfers between devices  145 us (55%)
  matrix products  66.4 us (25%)
  blocking collectives  19.4 us (7%)
  between operations  14 us (5%)
  local copies, waits for them, and re-layouts  9.67 us (4%)
  other arithmetic  8.34 us (3%)
    reduce_scatter x1, waiting for transfers between devices, per_device(): lax.psum_scatter(batched_f32(later_product, local_b), 'sp', scatter_dimen...  59.9 us
    all_gather x1, waiting for transfers between devices, prefix(): gathered = lax.all_gather(part, axis)  49.2 us
    all_gather x1, waiting for transfers between devices, per_device(): piece = lax.all_gather(tokens, 'tp', axis=1, tiled=True)  35.6 us
    psum x1, blocking collectives, per_device(): raw_read = lax.psum(partial_read, 'sp')  19.4 us
    dot_general x13, matrix products, matmul_f32(): return jnp.dot(left, right, precision=lax.Precision.HIGHEST)  18.7 us
    dot_general x8, matrix products, advance(): jnp.einsum('hcd,hce->hde', key_remainder, fresh, precision=lax.Precision....  13.2 us
    dot_general x8, matrix products, batched_f32(): jnp.einsum('hij,hjk->hik', left, right, precision=lax.Precision.HIGHEST)  12.2 us
    dot_general x8, matrix products, advance(): jnp.einsum('hcd,hde->hce', erase, state, precision=lax.Precision.HIGHEST)  10.7 us
  transfers between devices with their start and end apart: 3, of which 3 were waited for; matrix products, arithmetic and copies ran while one was open for 1% of the time, Pallas kernels for 0%

commit v1 on v0

v1 whole, which is shorter than its diff:
```python
import functools

import jax
import jax.numpy as jnp
from jax import lax
from jax.experimental import pallas as pl
from jax.experimental.pallas import tpu as pltpu
from jax.sharding import PartitionSpec as P

DK = 128
DV = 128
CHUNK = 128
LANES = 128
SUB = 8
norm_eps = 1e-06
MESH = pl.DeviceIdType.MESH
F32 = jnp.float32
BF16 = jnp.bfloat16


def mm(left, right):
    return jnp.dot(left.astype(BF16), right.astype(BF16), preferred_element_type=F32)


def mm_nt(left, right):
    return lax.dot_general(
        left.astype(BF16), right.astype(BF16), (((1,), (1,)), ((), ())), preferred_element_type=F32
    )


def log2(value):
    return value.bit_length() - 1


def body(
    n_sp,
    n_tp,
    x_ref,
    wk_hbm,
    wv_hbm,
    wb_hbm,
    wd_hbm,
    bias_ref,
    rate_ref,
    finc_ref,
    q_ref,
    gain_ref,
    state_out,
    read_out,
    wk,
    wv,
    wb,
    wd,
    wg,
    xg,
    acck,
    accv,
    accg,
    maps,
    gams,
    sendbuf,
    recvbuf,
    gsend,
    grecv,
    qslots,
    fstate,
    srecv,
    fread,
    rrecv,
    wsem,
    own_send,
    peer_send,
    fwd_send,
    tok_recv,
    q_send,
    q_recv,
    map_send,
    map_recv,
    g_send,
    g_recv,
    s_send,
    s_recv,
    r_send,
    r_recv,
):
    sp = lax.axis_index("sp")
    tp = lax.axis_index("tp")
    tokens_here, features = x_ref.shape
    heads = wk.shape[1] // DK
    chunks = tokens_here // CHUNK
    n_y = n_tp // 2
    y = tp // 2
    core = tp % 2
    sibling = tp + 1 - 2 * core
    levels = log2(n_sp)
    rows_out = DK // n_sp

    loads = [
        pltpu.make_async_copy(wk_hbm, wk, wsem.at[0]),
        pltpu.make_async_copy(wv_hbm, wv, wsem.at[1]),
        pltpu.make_async_copy(wb_hbm, wb, wsem.at[2]),
        pltpu.make_async_copy(wd_hbm, wd, wsem.at[3]),
    ]
    for load in (loads[2], loads[3], loads[0], loads[1]):
        load.start()

    barrier = pltpu.get_barrier_semaphore()
    pl.semaphore_signal(barrier, inc=1, device_id={"tp": sibling}, device_id_type=MESH)
    for step in range(1, n_y):
        peer = ((y + step) % n_y) * 2 + core
        pl.semaphore_signal(barrier, inc=1, device_id={"tp": peer}, device_id_type=MESH)
    for step in range(1, n_sp):
        pl.semaphore_signal(
            barrier, inc=1, device_id={"sp": (sp + step) % n_sp}, device_id_type=MESH
        )
    pl.semaphore_wait(barrier, n_y + n_sp - 1)

    def rows_of(c):
        return pl.ds(c * CHUNK, CHUNK)

    def copy_own(c):
        return pltpu.make_async_remote_copy(
            src_ref=x_ref.at[rows_of(c)],
            dst_ref=xg.at[tp, rows_of(c)],
            send_sem=own_send.at[c],
            recv_sem=tok_recv.at[tp, c],
            device_id={"tp": sibling},
            device_id_type=MESH,
        )

    def copy_peer(step, c):
        peer = ((y + step) % n_y) * 2 + core
        return pltpu.make_async_remote_copy(
            src_ref=x_ref.at[rows_of(c)],
            dst_ref=xg.at[tp, rows_of(c)],
            send_sem=peer_send.at[step, c],
            recv_sem=tok_recv.at[tp, c],
            device_id={"tp": peer},
            device_id_type=MESH,
        )

    def copy_forward(step, c):
        source = ((y + n_y - step) % n_y) * 2 + core
        return pltpu.make_async_remote_copy(
            src_ref=xg.at[source, rows_of(c)],
            dst_ref=xg.at[source, rows_of(c)],
            send_sem=fwd_send.at[step, c],
            recv_sem=tok_recv.at[source, c],
            device_id={"tp": sibling},
            device_id_type=MESH,
        )

    def arrived(source, c):
        pltpu.make_async_remote_copy(
            src_ref=xg.at[source, rows_of(c)],
            dst_ref=xg.at[source, rows_of(c)],
            send_sem=own_send.at[c],
            recv_sem=tok_recv.at[source, c],
            device_id={"tp": sibling},
            device_id_type=MESH,
        ).wait_recv()

    for c in range(chunks):
        for step in range(1, n_y):
            copy_peer(step, c).start()
        copy_own(c).start()

    def copy_query(step):
        return pltpu.make_async_remote_copy(
            src_ref=q_ref,
            dst_ref=qslots.at[sp],
            send_sem=q_send.at[step],
            recv_sem=q_recv.at[sp],
            device_id={"sp": (sp + step) % n_sp},
            device_id_type=MESH,
        )

    for step in range(1, n_sp):
        copy_query(step).start()

    total_heads = wb.shape[1]
    row_id = lax.broadcasted_iota(jnp.int32, (total_heads, LANES), 0)
    lane_id = lax.broadcasted_iota(jnp.int32, (total_heads, LANES), 1)
    first_head = tp * heads
    pick_b = jnp.where((row_id == lane_id + first_head) & (lane_id < heads), 1.0, 0.0)
    pick_d = jnp.where(
        (row_id == lane_id - SUB + first_head) & (lane_id >= SUB) & (lane_id < SUB + heads),
        1.0,
        0.0,
    )
    loads[2].wait()
    loads[3].wait()
    depth = wg.shape[0]
    piece = 512

    def pick(step, carry):
        rows = pl.ds(pl.multiple_of(step * piece, piece), piece)
        wg[rows, :] = (mm(wb[rows, :], pick_b) + mm(wd[rows, :], pick_d)).astype(BF16)
        return carry

    lax.fori_loop(0, depth // piece, pick, 0)
    loads[0].wait()
    loads[1].wait()

    def project(x, source, rows, first=False):
        deep = pl.ds(pl.multiple_of(source * features, features), features)
        for acc, weights in ((acck, wk), (accv, wv), (accg, wg)):
            part = jnp.dot(x, weights[deep, :], preferred_element_type=F32)
            acc[rows, :] = part if first else acc[rows, :] + part

    half_rows = 256 if tokens_here % 256 == 0 else CHUNK

    def own_project(step, carry):
        rows = pl.ds(pl.multiple_of(step * half_rows, half_rows), half_rows)
        project(x_ref[rows, :], tp, rows, True)
        return carry

    lax.fori_loop(0, tokens_here // half_rows, own_project, 0)
    for c in range(chunks):
        arrived(sibling, c)

    def sibling_project(step, carry):
        rows = pl.ds(pl.multiple_of(step * half_rows, half_rows), half_rows)
        project(xg[sibling, rows, :], sibling, rows)
        return carry

    lax.fori_loop(0, tokens_here // half_rows, sibling_project, 0)

    row8 = lax.broadcasted_iota(jnp.int32, (SUB, total_heads), 0)
    lane8 = lax.broadcasted_iota(jnp.int32, (SUB, total_heads), 1)
    mine = (lane8 == row8 + first_head) & (row8 < heads)
    bias_col = jnp.sum(jnp.where(mine, bias_ref[...], 0.0), axis=1, keepdims=True)
    rate_col = jnp.sum(jnp.where(mine, rate_ref[...], 0.0), axis=1, keepdims=True)

    maps[...] = jnp.zeros_like(maps)
    gams[...] = jnp.ones_like(gams)

    def chunk_step(c, carry):
        rows = pl.ds(pl.multiple_of(c * CHUNK, CHUNK), CHUNK)
        for step in range(1, n_y):
            arrived(((y + n_y - step) % n_y) * 2 + core, c)
            copy_forward(step, c).start()
        for step in range(1, n_y):
            source = ((y + n_y - step) % n_y) * 2 + core
            project(xg[source, rows, :], source, rows)
        for step in range(1, n_y):
            source = ((y + n_y - step) % n_y) * 2 + 1 - core
            arrived(source, c)
            project(xg[source, rows, :], source, rows)

        ri = lax.broadcasted_iota(jnp.int32, (CHUNK, CHUNK), 0)
        ci = lax.broadcasted_iota(jnp.int32, (CHUNK, CHUNK), 1)
        strict = ri > ci
        upper = jnp.where(ri <= ci, 1.0, 0.0)
        gates = jnp.transpose(accg[rows, :])
        beta = jax.nn.sigmoid(gates[0:SUB, :] + bias_col)
        raw = gates[SUB : 2 * SUB, :]
        softplus = jnp.maximum(raw, 0.0) + jnp.log1p(jnp.exp(-jnp.abs(raw)))
        logd = -rate_col * softplus + finc_ref[:, rows]
        cum = jnp.dot(logd, upper, precision=lax.Precision.HIGHEST, preferred_element_type=F32)
        total = jnp.sum(logd, axis=1, keepdims=True)
        columns = jnp.transpose(
            jnp.concatenate(
                [
                    beta,
                    cum,
                    jnp.exp(cum),
                    jnp.exp(total - cum),
                    jnp.zeros((LANES - 4 * SUB, LANES), F32),
                ],
                axis=0,
            )
        )
        keep = jnp.exp(total)

        keys, rights, powers, remains = [], [], [], []
        for h in range(heads):
            cols = slice(h * DK, (h + 1) * DK)
            key = acck[rows, cols].astype(BF16).astype(F32)
            key = key * lax.rsqrt(jnp.sum(key * key, axis=-1, keepdims=True) + norm_eps)
            value = accv[rows, cols].astype(BF16).astype(F32)
            b_col = columns[:, h : h + 1]
            c_col = columns[:, SUB + h : SUB + h + 1]
            e_col = columns[:, 2 * SUB + h : 2 * SUB + h + 1]
            r_col = columns[:, 3 * SUB + h : 3 * SUB + h + 1]
            key_beta = key * b_col
            decay = jnp.exp(jnp.where(strict, c_col - cum[h : h + 1, :], 0.0))
            powers.append(jnp.where(strict, mm_nt(key_beta, key) * decay, 0.0))
            rights.append(jnp.concatenate([value * b_col, key_beta * e_col], axis=1))
            remains.append(jnp.transpose(key * r_col))
        solved = [rights[h] - mm(powers[h], rights[h]) for h in range(heads)]
        covered = 2
        while covered < CHUNK:
            powers = [mm(power, power) for power in powers]
            solved = [solved[h] + mm(powers[h], solved[h]) for h in range(heads)]
            covered *= 2
        fresh = []
        for h in range(heads):
            gamma = gams[h, 0:1, 0:1]
            erase = solved[h][:, DV:]
            direct = jnp.concatenate([solved[h][:, :DV], -gamma * erase], axis=1)
            fresh.append(direct - mm(erase, maps[h]))
        for h in range(heads):
            maps[h] = keep[h : h + 1, :] * maps[h] + mm(remains[h], fresh[h])
            gams[h] = keep[h : h + 1, :] * gams[h]
        return carry

    lax.fori_loop(0, chunks, chunk_step, 0)

    count = heads
    offset = 0
    my_head = 0
    for level in range(levels):
        bit = (sp // (1 << level)) % 2
        partner = sp + (1 - 2 * bit) * (1 << level)
        split = count > 1
        half = count // 2 if split else count
        keep_at = my_head + (bit * half if split else 0)
        send_at = my_head + ((1 - bit) * half if split else 0)
        rows = pl.ds(offset, half)
        for i in range(half):
            sendbuf[offset + i] = maps[send_at + i].astype(BF16)
            gsend[offset + i] = gams[send_at + i]
        move = pltpu.make_async_remote_copy(
            src_ref=sendbuf.at[rows],
            dst_ref=recvbuf.at[rows],
            send_sem=map_send.at[level],
            recv_sem=map_recv.at[level],
            device_id={"sp": partner},
            device_id_type=MESH,
        )
        move_g = pltpu.make_async_remote_copy(
            src_ref=gsend.at[rows],
            dst_ref=grecv.at[rows],
            send_sem=g_send.at[level],
            recv_sem=g_recv.at[level],
            device_id={"sp": partner},
            device_id_type=MESH,
        )
        move.start()
        move_g.start()
        move.wait()
        move_g.wait()
        later = bit == 1
        for i in range(half):
            own = maps[keep_at + i]
            if not split:
                own = own.astype(BF16).astype(F32)
            own_g = gams[keep_at + i]
            got = recvbuf[offset + i].astype(F32)
            got_g = grecv[offset + i]
            left = jnp.where(later, own, got)
            left_g = jnp.where(later, own_g, got_g)
            right = jnp.where(later, got, own)
            right_g = jnp.where(later, got_g, own_g)
            tail = left[:, DV:]
            added = jnp.concatenate([left[:, :DV], right_g[0:1, 0:1] * tail], axis=1)
            maps[keep_at + i] = left_g[0:1, 0:1] * right + mm(tail, right) + added
            gams[keep_at + i] = left_g * right_g
        offset += half
        count = half
        my_head = keep_at

    final = maps[my_head][:, :DV]
    for j in range(n_sp):
        fstate[j] = final[j * rows_out : (j + 1) * rows_out, :].astype(BF16)

    member = sp % heads
    base = sp - member

    def head_of(index):
        found = 0
        for place in range(log2(heads)):
            found = found * 2 + (index // (1 << place)) % 2
        return found

    def copy_state(step):
        target = base + (member + step) % heads
        return pltpu.make_async_remote_copy(
            src_ref=fstate.at[target],
            dst_ref=srecv.at[my_head],
            send_sem=s_send.at[step],
            recv_sem=s_recv.at[my_head],
            device_id={"sp": target},
            device_id_type=MESH,
        )

    for step in range(1, heads):
        copy_state(step).start()
    srecv[my_head] = fstate[sp]

    for step in range(1, n_sp):
        source = (sp + n_sp - step) % n_sp
        pltpu.make_async_remote_copy(
            src_ref=q_ref,
            dst_ref=qslots.at[source],
            send_sem=q_send.at[step],
            recv_sem=q_recv.at[source],
            device_id={"sp": source},
            device_id_type=MESH,
        ).wait_recv()
    qslots[sp] = q_ref[...]
    query = jnp.sum(qslots[...], axis=0)
    reads = mm(query, final)
    row_head = lax.broadcasted_iota(jnp.int32, (SUB, DV), 0)
    raw_read = jnp.sum(jnp.where(row_head == my_head, reads, 0.0), axis=0, keepdims=True)
    read = (
        raw_read
        * lax.rsqrt(jnp.mean(raw_read * raw_read, axis=-1, keepdims=True) + norm_eps)
        * gain_ref[...].astype(F32)
    )
    fread[...] = jnp.broadcast_to(read, fread.shape)

    def copy_read(step):
        target = base + (member + step) % heads
        return pltpu.make_async_remote_copy(
            src_ref=fread,
            dst_ref=rrecv.at[my_head],
            send_sem=r_send.at[step],
            recv_sem=r_recv.at[my_head],
            device_id={"sp": target},
            device_id_type=MESH,
        )

    for step in range(1, heads):
        copy_read(step).start()
    rrecv[my_head] = fread[...]

    for step in range(1, heads):
        other = (member + heads - step) % heads
        source = base + other
        head = head_of(other)
        pltpu.make_async_remote_copy(
            src_ref=fstate.at[source],
            dst_ref=srecv.at[head],
            send_sem=s_send.at[step],
            recv_sem=s_recv.at[head],
            device_id={"sp": source},
            device_id_type=MESH,
        ).wait_recv()
        pltpu.make_async_remote_copy(
            src_ref=fread,
            dst_ref=rrecv.at[head],
            send_sem=r_send.at[step],
            recv_sem=r_recv.at[head],
            device_id={"sp": source},
            device_id_type=MESH,
        ).wait_recv()
    for h in range(heads):
        state_out[h] = srecv[h]
        read_out[h : h + 1, :] = rrecv[h, 0:1, :]

    for c in range(chunks):
        copy_own(c).wait_send()
        for step in range(1, n_y):
            copy_peer(step, c).wait_send()
            copy_forward(step, c).wait_send()
    for step in range(1, n_sp):
        copy_query(step).wait_send()
    for step in range(1, heads):
        copy_state(step).wait_send()
        copy_read(step).wait_send()


def per_device(
    n_sp,
    n_tp,
    tokens,
    w_key,
    w_value,
    w_beta,
    w_decay,
    beta_bias,
    decay_rate,
    forgetting_increment,
    new_query,
    read_gain,
):
    tokens_here, features = tokens.shape
    depth, width = w_key.shape
    heads = width // DK
    chunks = tokens_here // CHUNK
    rows_out = DK // n_sp
    n_y = n_tp // 2
    levels = log2(n_sp)
    slots = 0
    count = heads
    for _ in range(levels):
        count = max(count // 2, 1)
        slots += count
    query = lax.dynamic_update_slice(
        jnp.zeros((SUB, DK), F32),
        new_query.astype(F32),
        (0, lax.axis_index("sp") * rows_out),
    )
    increments = jnp.pad(forgetting_increment, ((0, SUB - heads), (0, 0)))
    vmem = pl.BlockSpec(memory_space=pltpu.VMEM)
    hbm = pl.BlockSpec(memory_space=pl.ANY)
    dma = pltpu.SemaphoreType.DMA
    return pl.pallas_call(
        functools.partial(body, n_sp, n_tp),
        name="delta_state",
        out_shape=(
            jax.ShapeDtypeStruct((heads, rows_out, DV), BF16),
            jax.ShapeDtypeStruct((heads, DV), F32),
        ),
        in_specs=[vmem, hbm, hbm, hbm, hbm, vmem, vmem, vmem, vmem, vmem],
        out_specs=(vmem, vmem),
        scratch_shapes=[
            pltpu.VMEM((depth, width), BF16),
            pltpu.VMEM((depth, width), BF16),
            pltpu.VMEM(w_beta.shape, BF16),
            pltpu.VMEM(w_decay.shape, BF16),
            pltpu.VMEM((depth, LANES), BF16),
            pltpu.VMEM((n_tp, tokens_here, features), BF16),
            pltpu.VMEM((tokens_here, width), F32),
            pltpu.VMEM((tokens_here, width), F32),
            pltpu.VMEM((tokens_here, LANES), F32),
            pltpu.VMEM((heads, DK, DV + DK), F32),
            pltpu.VMEM((heads, SUB, LANES), F32),
            pltpu.VMEM((slots, DK, DV + DK), BF16),
            pltpu.VMEM((slots, DK, DV + DK), BF16),
            pltpu.VMEM((slots, SUB, LANES), F32),
            pltpu.VMEM((slots, SUB, LANES), F32),
            pltpu.VMEM((n_sp, SUB, DK), F32),
            pltpu.VMEM((n_sp, rows_out, DV), BF16),
            pltpu.VMEM((heads, rows_out, DV), BF16),
            pltpu.VMEM((SUB, DV), F32),
            pltpu.VMEM((heads, SUB, DV), F32),
            dma((4,)),
            dma((chunks,)),
            dma((n_y, chunks)),
            dma((n_y, chunks)),
            dma((n_tp, chunks)),
            dma((n_sp,)),
            dma((n_sp,)),
            dma((levels,)),
            dma((levels,)),
            dma((levels,)),
            dma((levels,)),
            dma((heads,)),
            dma((heads,)),
            dma((heads,)),
            dma((heads,)),
        ],
        compiler_params=pltpu.CompilerParams(
            collective_id=0, has_side_effects=True, vmem_limit_bytes=60 * 1024 * 1024
        ),
    )(
        tokens,
        w_key,
        w_value,
        w_beta,
        w_decay,
        beta_bias[None, :],
        decay_rate[None, :],
        increments,
        query,
        read_gain[None, :],
    )


def solution(mesh):
    return jax.shard_map(
        functools.partial(per_device, mesh.shape["sp"], mesh.shape["tp"]),
        mesh=mesh,
        in_specs=(
            P("sp", "tp"),
            P(None, "tp"),
            P(None, "tp"),
            P(),
            P(),
            P(),
            P(),
            P("tp", "sp"),
            P("tp", "sp"),
            P(),
        ),
        out_specs=(P("tp", "sp", None), P("tp", None)),
        check_vma=False,
    )
```

time: 265 us -> 63.1 us (0.24)
  waiting for transfers between devices: 145 us -> 0 us
  matrix products: 66.4 us -> 0 us
  Pallas kernels: 0 us -> 52.9 us
  blocking collectives: 19.4 us -> 0 us
  between operations: 14 us -> 0.66 us
  other arithmetic: 8.34 us -> 0.68 us
    all_gather x2 -> x0, waiting for transfers between devices: 84.8 us -> none  [the longest x1 49.2 us: prefix(): gathered = lax.all_gather(part, axis)]
    dot_general x40 -> x0, matrix products: 66.4 us -> none  [the longest x13 18.7 us: matmul_f32(): return jnp.dot(left, right, precision=lax.Precision.HIGHEST)]
    reduce_scatter x1 -> x0, waiting for transfers between devices: 59.9 us -> none  [per_device(): lax.psum_scatter(batched_f32(later_product, local_b), 'sp', scatter_dimen...]
    pallas_call x0 -> x1, Pallas kernels: none -> 52.9 us  [per_device(): pl.pallas_call(functools.partial(body, n_sp, n_tp), name='delta_state', o...]
    psum x1 -> x0, blocking collectives: 19.4 us -> none  [per_device(): raw_read = lax.psum(partial_read, 'sp')]
    unnamed x11 -> x6, local copies, waits for them, and re-layouts: 0.11 us -> 7.07 us
    mul x9 -> x0, local copies, waits for them, and re-layouts: 5.54 us -> none  [the longest x8 5.46 us: advance(): keep[:, None, None] * state]
  transfers between devices with their start and end apart: 3 -> 0, of which waited for: 3 -> 0; matrix products, arithmetic and copies ran while one was open for 1% -> 0% of each run, Pallas kernels for 0% -> 0%
where the time goes in v1:
time: 63.1 us; the launch traced here: 62.8 us
  Pallas kernels  52.9 us (84%)
  local copies, waits for them, and re-layouts  8.59 us (14%)
  other arithmetic  0.68 us (1%)
  between operations  0.66 us (1%)
    pallas_call x1, Pallas kernels, per_device(): pl.pallas_call(functools.partial(body, n_sp, n_tp), name='delta_state', o...  52.9 us
    unnamed x6, local copies, waits for them, and re-layouts  7.07 us
    pad x1, local copies, waits for them, and re-layouts, per_device(): increments = jnp.pad(forgetting_increment, ((0, SUB - heads), (0, 0)))  1.31 us

profile of v1, /device:TPU:0, one launch (start us, length us, event | category | flops | bytes accessed | tf_op | source)
XLA Modules:
  0.0 62.8 jit_solution(733184261111687010)
XLA Ops:
  0.6 0.7 %convert_element_type.5 = f32[4,16]{1,0:T(4,128)S(1)} convert(bf16[4,16]{1,0:T(4,128)(2,1)} %param.18) | non-fusion elementwise | flops 64 | bytes 384 | tf_op jit(solution)/shard_map/convert_element_type | solution.py:493
  1.3 0.2 dynamic_update_slice.3.q_ref
  1.5 0.0 copy-start
  1.5 1.3 %pad.4.finc_ref = f32[8,512]{1,0:T(8,128)} pad(f32[4,512]{1,0:T(4,128)} %param.17, f32[]{:T(128)} %constant.3.clone.1), padding=0_4x0_0 | pad | bytes 24580 | tf_op jit(solution)/shard_map/jit(_pad)/pad | solution.py:496
  2.9 2.2 %copy.12.wb_hbm = bf16[4096,16]{1,0:T(8,128)(2,1)} copy(bf16[4096,16]{0,1:T(8,128)(2,1)} %param.13) | data formatting | bytes 262144 | tf_op args[3]
  5.1 2.3 %copy.13.wd_hbm = bf16[4096,16]{1,0:T(8,128)(2,1)} copy(bf16[4096,16]{0,1:T(8,128)(2,1)} %param.14) | data formatting | bytes 262144 | tf_op args[4]
  7.4 0.0 copy-done
  7.4 52.9 %delta_state.1 = (bf16[4,16,128]{2,1,0:T(8,128)(2,1)}, f32[4,128]{1,0:T(4,128)}) custom-call(bf16[512,1024]{1,0:T(8,128)(2,1)} %x_ref.1, bf16[4096,512]{1,0:T(8,128)(2,1)} %wk_hbm.1, bf16[4096,512]{1,0:T(8,128)(2,1)} %wv_hbm.1, bf16[4096,16]{1,0:T(8,128)(2,1)} %copy.12.wb_hbm, bf16[4096,16]{1,0:T(8,128)(2,1)} %copy.13.wd_hbm, f32[1,16]{1,0:T(1,128)} %bitcast.3, ...), custom_call_target="tpu_custom_call" | custom-call | tf_op jit(solution)/shard_map/delta_state/pallas_call | solution.py:500
  60.2 1.3 %copy.17 = bf16[4,16,128]{2,1,0:T(8,128)(2,1)} copy(bf16[4,16,128]{2,1,0:T(8,128)(2,1)} %get-tuple-element.4) | data formatting | bytes 32768
  61.5 1.2 %copy.18 = f32[4,128]{1,0:T(4,128)} copy(f32[4,128]{1,0:T(4,128)} %get-tuple-element.5) | data formatting | bytes 4096
  (1 shorter events, 0.0 us)
Async XLA Ops:
  1.5 5.8 %copy-start = (f32[8,128]{1,0:T(8,128)}, f32[8,128]{1,0:T(8,128)S(1)}, u32[]{:S(2)}) copy-start(f32[8,128]{1,0:T(8,128)S(1)} %dynamic_update_slice.3.q_ref) | copy-start | bytes 12292

commit v2 on v1

--- a/solution.py
+++ b/solution.py
@@ -32,10 +32,14 @@
     return value.bit_length() - 1
 
 
+def tail_pieces(features):
+    return 4 if features % 1024 == 0 else 1
+
+
 def body(
     n_sp,
     n_tp,
-    x_ref,
+    x_hbm,
     wk_hbm,
     wv_hbm,
     wb_hbm,
@@ -52,6 +56,9 @@
     wb,
     wd,
     wg,
+    x_ref,
+    finc8,
+    q_own,
     xg,
     acck,
     accv,
@@ -88,6 +95,10 @@
     tokens_here, features = x_ref.shape
     heads = wk.shape[1] // DK
     chunks = tokens_here // CHUNK
+    last = chunks - 1
+    pieces = tail_pieces(features)
+    wide = features // pieces
+    parts = last + pieces
     n_y = n_tp // 2
     y = tp // 2
     core = tp % 2
@@ -95,6 +106,8 @@
     levels = log2(n_sp)
     rows_out = DK // n_sp
 
+    load_x = pltpu.make_async_copy(x_hbm, x_ref, wsem.at[4])
+    load_x.start()
     loads = [
         pltpu.make_async_copy(wk_hbm, wk, wsem.at[0]),
         pltpu.make_async_copy(wv_hbm, wv, wsem.at[1]),
@@ -109,85 +122,103 @@
     for step in range(1, n_y):
         peer = ((y + step) % n_y) * 2 + core
         pl.semaphore_signal(barrier, inc=1, device_id={"tp": peer}, device_id_type=MESH)
-    for step in range(1, n_sp):
-        pl.semaphore_signal(
-            barrier, inc=1, device_id={"sp": (sp + step) % n_sp}, device_id_type=MESH
-        )
-    pl.semaphore_wait(barrier, n_y + n_sp - 1)
-
-    def rows_of(c):
-        return pl.ds(c * CHUNK, CHUNK)
-
-    def copy_own(c):
+    masks = sorted(set(range(1, heads)) | {1 << level for level in range(levels)})
+
+    def flip(mask):
+        found = sp
+        for place in range(levels):
+            if (mask >> place) % 2:
+                found = found + (1 - 2 * ((sp // (1 << place)) % 2)) * (1 << place)
+        return found
+
+    for mask in masks:
+        pl.semaphore_signal(barrier, inc=1, device_id={"sp": flip(mask)}, device_id_type=MESH)
+
+    def part_of(k):
+        if isinstance(k, int) and k >= last:
+            return pl.ds(last * CHUNK, CHUNK), pl.ds((k - last) * wide, wide)
+        start = k * CHUNK if isinstance(k, int) else pl.multiple_of(k * CHUNK, CHUNK)
+        return pl.ds(start, CHUNK), pl.ds(0, features)
+
+    def copy_own(k):
+        rows, cols = part_of(k)
         return pltpu.make_async_remote_copy(
-            src_ref=x_ref.at[rows_of(c)],
-            dst_ref=xg.at[tp, rows_of(c)],
-            send_sem=own_send.at[c],
-            recv_sem=tok_recv.at[tp, c],
+            src_ref=x_ref.at[rows, cols],
+            dst_ref=xg.at[tp, rows, cols],
+            send_sem=own_send.at[k],
+            recv_sem=tok_recv.at[tp, k],
             device_id={"tp": sibling},
             device_id_type=MESH,
         )
 
-    def copy_peer(step, c):
+    def copy_peer(step, k):
+        rows, cols = part_of(k)
         peer = ((y + step) % n_y) * 2 + core
         return pltpu.make_async_remote_copy(
-            src_ref=x_ref.at[rows_of(c)],
-            dst_ref=xg.at[tp, rows_of(c)],
-            send_sem=peer_send.at[step, c],
-            recv_sem=tok_recv.at[tp, c],
+            src_ref=x_ref.at[rows, cols],
+            dst_ref=xg.at[tp, rows, cols],
+            send_sem=peer_send.at[step, k],
+            recv_sem=tok_recv.at[tp, k],
             device_id={"tp": peer},
             device_id_type=MESH,
         )
 
-    def copy_forward(step, c):
+    def copy_forward(step, k):
+        rows, cols = part_of(k)
         source = ((y + n_y - step) % n_y) * 2 + core
         return pltpu.make_async_remote_copy(
-            src_ref=xg.at[source, rows_of(c)],
-            dst_ref=xg.at[source, rows_of(c)],
-            send_sem=fwd_send.at[step, c],
-            recv_sem=tok_recv.at[source, c],
+            src_ref=xg.at[source, rows, cols],
+            dst_ref=xg.at[source, rows, cols],
+            send_sem=fwd_send.at[step, k],
+            recv_sem=tok_recv.at[source, k],
             device_id={"tp": sibling},
             device_id_type=MESH,
         )
 
-    def arrived(source, c):
+    def arrived(source, k):
+        rows, cols = part_of(k)
         pltpu.make_async_remote_copy(
-            src_ref=xg.at[source, rows_of(c)],
-            dst_ref=xg.at[source, rows_of(c)],
-            send_sem=own_send.at[c],
-            recv_sem=tok_recv.at[source, c],
+            src_ref=xg.at[source, rows, cols],
+            dst_ref=xg.at[source, rows, cols],
+            send_sem=own_send.at[k],
+            recv_sem=tok_recv.at[source, k],
             device_id={"tp": sibling},
             device_id_type=MESH,
         ).wait_recv()
 
-    for c in range(chunks):
-        for step in range(1, n_y):
-            copy_peer(step, c).start()
-        copy_own(c).start()
-
-    def copy_query(step):
-        return pltpu.make_async_remote_copy(
-            src_ref=q_ref,
-            dst_ref=qslots.at[sp],
-            send_sem=q_send.at[step],
-            recv_sem=q_recv.at[sp],
-            device_id={"sp": (sp + step) % n_sp},
-            device_id_type=MESH,
-        )
-
-    for step in range(1, n_sp):
-        copy_query(step).start()
-
-    total_heads = wb.shape[1]
-    row_id = lax.broadcasted_iota(jnp.int32, (total_heads, LANES), 0)
-    lane_id = lax.broadcasted_iota(jnp.int32, (total_heads, LANES), 1)
+    pl.semaphore_wait(barrier, n_y + len(masks))
+    load_x.wait()
+    for k in range(parts):
+        for step in range(1, n_y):
+            copy_peer(step, k).start()
+        copy_own(k).start()
+
+    rows_q = lax.broadcasted_iota(jnp.int32, (rows_out, LANES), 0)
+    lanes_q = lax.broadcasted_iota(jnp.int32, (rows_out, LANES), 1)
+    place_q = jnp.where(lanes_q == rows_q + sp * rows_out, 1.0, 0.0)
+    q_own[...] = jnp.zeros_like(q_own)
+    q_own[0:heads, :] = mm(q_ref[...], place_q)
+    qslots[sp] = q_own[...]
+
+    lead = heads // 2
+    bit0 = sp % 2
+
+    def actual(i):
+        return (i + (1 - bit0) * lead) % heads if heads > 1 else i
+
+    finc8[...] = jnp.zeros_like(finc8)
+    for i in range(heads):
+        finc8[i : i + 1, :] = finc_ref[pl.ds(actual(i), 1), :]
+
+    total_heads = wb.shape[0]
+    row_id = lax.broadcasted_iota(jnp.int32, (LANES, total_heads), 0)
+    col_id = lax.broadcasted_iota(jnp.int32, (LANES, total_heads), 1)
     first_head = tp * heads
-    pick_b = jnp.where((row_id == lane_id + first_head) & (lane_id < heads), 1.0, 0.0)
-    pick_d = jnp.where(
-        (row_id == lane_id - SUB + first_head) & (lane_id >= SUB) & (lane_id < SUB + heads),
-        1.0,
-        0.0,
-    )
+    shift = (1 - bit0) * lead
+    own_head = first_head + (row_id % SUB + shift) % heads
+    own = (row_id % SUB < heads) & (col_id == own_head)
+    pick_b = jnp.where(own & (row_id < SUB), 1.0, 0.0)
+    pick_d = jnp.where(own & (row_id >= SUB) & (row_id < 2 * SUB), 1.0, 0.0)
     loads[2].wait()
     loads[3].wait()
     depth = wg.shape[0]
@@ -195,15 +226,16 @@
 
     def pick(step, carry):
         rows = pl.ds(pl.multiple_of(step * piece, piece), piece)
-        wg[rows, :] = (mm(wb[rows, :], pick_b) + mm(wd[rows, :], pick_d)).astype(BF16)
+        both = mm(pick_b, wb[:, rows]) + mm(pick_d, wd[:, rows])
+        wg[rows, :] = jnp.transpose(both).astype(BF16)
         return carry
 
     lax.fori_loop(0, depth // piece, pick, 0)
     loads[0].wait()
     loads[1].wait()
 
-    def project(x, source, rows, first=False):
-        deep = pl.ds(pl.multiple_of(source * features, features), features)
+    def project(x, source, rows, first=False, start=0, size=features):
+        deep = pl.ds(pl.multiple_of(source * features + start, size), size)
         for acc, weights in ((acck, wk), (accv, wv), (accg, wg)):
             part = jnp.dot(x, weights[deep, :], preferred_element_type=F32)
             acc[rows, :] = part if first else acc[rows, :] + part
@@ -216,8 +248,8 @@
         return carry
 
     lax.fori_loop(0, tokens_here // half_rows, own_project, 0)
-    for c in range(chunks):
-        arrived(sibling, c)
+    for k in range(parts):
+        arrived(sibling, k)
 
     def sibling_project(step, carry):
         rows = pl.ds(pl.multiple_of(step * half_rows, half_rows), half_rows)
@@ -228,26 +260,20 @@
 
     row8 = lax.broadcasted_iota(jnp.int32, (SUB, total_heads), 0)
     lane8 = lax.broadcasted_iota(jnp.int32, (SUB, total_heads), 1)
-    mine = (lane8 == row8 + first_head) & (row8 < heads)
+    mine = (lane8 == first_head + (row8 + shift) % heads) & (row8 < heads)
     bias_col = jnp.sum(jnp.where(mine, bias_ref[...], 0.0), axis=1, keepdims=True)
     rate_col = jnp.sum(jnp.where(mine, rate_ref[...], 0.0), axis=1, keepdims=True)
 
     maps[...] = jnp.zeros_like(maps)
     gams[...] = jnp.ones_like(gams)
 
-    def chunk_step(c, carry):
-        rows = pl.ds(pl.multiple_of(c * CHUNK, CHUNK), CHUNK)
-        for step in range(1, n_y):
-            arrived(((y + n_y - step) % n_y) * 2 + core, c)
-            copy_forward(step, c).start()
-        for step in range(1, n_y):
-            source = ((y + n_y - step) % n_y) * 2 + core
-            project(xg[source, rows, :], source, rows)
-        for step in range(1, n_y):
-            source = ((y + n_y - step) % n_y) * 2 + 1 - core
-            arrived(source, c)
-            project(xg[source, rows, :], source, rows)
-
+    def near(step):
+        return ((y + n_y - step) % n_y) * 2 + core
+
+    def far(step):
+        return ((y + n_y - step) % n_y) * 2 + 1 - core
+
+    def gate_terms(rows):
         ri = lax.broadcasted_iota(jnp.int32, (CHUNK, CHUNK), 0)
         ci = lax.broadcasted_iota(jnp.int32, (CHUNK, CHUNK), 1)
         strict = ri > ci
@@ -256,7 +282,7 @@
         beta = jax.nn.sigmoid(gates[0:SUB, :] + bias_col)
         raw = gates[SUB : 2 * SUB, :]
         softplus = jnp.maximum(raw, 0.0) + jnp.log1p(jnp.exp(-jnp.abs(raw)))
-        logd = -rate_col * softplus + finc_ref[:, rows]
+        logd = -rate_col * softplus + finc8[:, rows]
         cum = jnp.dot(logd, upper, precision=lax.Precision.HIGHEST, preferred_element_type=F32)
         total = jnp.sum(logd, axis=1, keepdims=True)
         columns = jnp.transpose(
@@ -271,11 +297,13 @@
                 axis=0,
             )
         )
-        keep = jnp.exp(total)
-
-        keys, rights, powers, remains = [], [], [], []
-        for h in range(heads):
-            cols = slice(h * DK, (h + 1) * DK)
+        return strict, cum, columns, jnp.exp(total)
+
+    def advance(rows, terms, chosen):
+        strict, cum, columns, keep = terms
+        rights, powers, remains = [], [], []
+        for h in chosen:
+            cols = pl.ds(pl.multiple_of(actual(h) * DK, DK), DK)
             key = acck[rows, cols].astype(BF16).astype(F32)
             key = key * lax.rsqrt(jnp.sum(key * key, axis=-1, keepdims=True) + norm_eps)
             value = accv[rows, cols].astype(BF16).astype(F32)
@@ -288,36 +316,80 @@
             powers.append(jnp.where(strict, mm_nt(key_beta, key) * decay, 0.0))
             rights.append(jnp.concatenate([value * b_col, key_beta * e_col], axis=1))
             remains.append(jnp.transpose(key * r_col))
-        solved = [rights[h] - mm(powers[h], rights[h]) for h in range(heads)]
+        solved = [right - mm(power, right) for power, right in zip(powers, rights)]
         covered = 2
         while covered < CHUNK:
             powers = [mm(power, power) for power in powers]
-            solved = [solved[h] + mm(powers[h], solved[h]) for h in range(heads)]
+            solved = [known + mm(power, known) for power, known in zip(powers, solved)]
             covered *= 2
         fresh = []
-        for h in range(heads):
+        for h, known in zip(chosen, solved):
             gamma = gams[h, 0:1, 0:1]
-            erase = solved[h][:, DV:]
-            direct = jnp.concatenate([solved[h][:, :DV], -gamma * erase], axis=1)
+            erase = known[:, DV:]
+            direct = jnp.concatenate([known[:, :DV], -gamma * erase], axis=1)
             fresh.append(direct - mm(erase, maps[h]))
-        for h in range(heads):
-            maps[h] = keep[h : h + 1, :] * maps[h] + mm(remains[h], fresh[h])
-            gams[h] = keep[h : h + 1, :] * gams[h]
+        for h, remain, new in zip(chosen, remains, fresh):
+            maps[h] = keep[h : h + 1, 0:1] * maps[h] + mm(remain, new)
+            gams[h] = keep[h : h + 1, 0:1] * gams[h]
+
+    def chunk_step(c, carry):
+        rows = pl.ds(pl.multiple_of(c * CHUNK, CHUNK), CHUNK)
+        for step in range(1, n_y):
+            arrived(near(step), c)
+            copy_forward(step, c).start()
+        for step in range(1, n_y):
+            project(xg[near(step), rows, :], near(step), rows)
+        for step in range(1, n_y):
+            arrived(far(step), c)
+            project(xg[far(step), rows, :], far(step), rows)
+        advance(rows, gate_terms(rows), range(heads))
         return carry
 
-    lax.fori_loop(0, chunks, chunk_step, 0)
+    lax.fori_loop(0, last, chunk_step, 0)
+
+    def far_part(k):
+        rows, cols = part_of(k)
+        for step in range(1, n_y):
+            arrived(far(step), k)
+            project(xg[far(step), rows, cols], far(step), rows, False, (k - last) * wide, wide)
+
+    end_rows = pl.ds(last * CHUNK, CHUNK)
+    for k in range(last, parts):
+        rows, cols = part_of(k)
+        for step in range(1, n_y):
+            arrived(near(step), k)
+            copy_forward(step, k).start()
+        for step in range(1, n_y):
+            project(xg[near(step), rows, cols], near(step), rows, False, (k - last) * wide, wide)
+        if k > last:
+            far_part(k - 1)
+    far_part(parts - 1)
+    end_terms = gate_terms(end_rows)
 
     count = heads
     offset = 0
-    my_head = 0
+    held = 0
     for level in range(levels):
         bit = (sp // (1 << level)) % 2
-        partner = sp + (1 - 2 * bit) * (1 << level)
+        partner = flip(1 << level)
         split = count > 1
         half = count // 2 if split else count
-        keep_at = my_head + (bit * half if split else 0)
-        send_at = my_head + ((1 - bit) * half if split else 0)
+        if level == 0:
+            send_at, keep_at = 0, heads - half
+            advance(end_rows, end_terms, range(half))
+        else:
+            keep_at = held + (bit * half if split else 0)
+            send_at = held + ((1 - bit) * half if split else 0)
         rows = pl.ds(offset, half)
+        known_q = pl.ds(sp - sp % (1 << level), 1 << level)
+        move_q = pltpu.make_async_remote_copy(
+            src_ref=qslots.at[known_q],
+            dst_ref=qslots.at[known_q],
+            send_sem=q_send.at[level],
+            recv_sem=q_recv.at[level],
+            device_id={"sp": partner},
+            device_id_type=MESH,
+        )
         for i in range(half):
             sendbuf[offset + i] = maps[send_at + i].astype(BF16)
             gsend[offset + i] = gams[send_at + i]
@@ -339,8 +411,12 @@
         )
         move.start()
         move_g.start()
+        move_q.start()
+        if level == 0 and split:
+            advance(end_rows, end_terms, range(half, heads))
         move.wait()
         move_g.wait()
+        move_q.wait()
         later = bit == 1
         for i in range(half):
             own = maps[keep_at + i]
@@ -359,14 +435,12 @@
             gams[keep_at + i] = left_g * right_g
         offset += half
         count = half
-        my_head = keep_at
-
-    final = maps[my_head][:, :DV]
+        held = keep_at
+
+    my_head = bit0 * lead + held - lead if heads > 1 else 0
+    final = maps[held][:, :DV]
     for j in range(n_sp):
         fstate[j] = final[j * rows_out : (j + 1) * rows_out, :].astype(BF16)
-
-    member = sp % heads
-    base = sp - member
 
     def head_of(index):
         found = 0
@@ -375,7 +449,7 @@
         return found
 
     def copy_state(step):
-        target = base + (member + step) % heads
+        target = flip(step)
         return pltpu.make_async_remote_copy(
             src_ref=fstate.at[target],
             dst_ref=srecv.at[my_head],
@@ -389,17 +463,6 @@
         copy_state(step).start()
     srecv[my_head] = fstate[sp]
 
-    for step in range(1, n_sp):
-        source = (sp + n_sp - step) % n_sp
-        pltpu.make_async_remote_copy(
-            src_ref=q_ref,
-            dst_ref=qslots.at[source],
-            send_sem=q_send.at[step],
-            recv_sem=q_recv.at[source],
-            device_id={"sp": source},
-            device_id_type=MESH,
-        ).wait_recv()
-    qslots[sp] = q_ref[...]
     query = jnp.sum(qslots[...], axis=0)
     reads = mm(query, final)
     row_head = lax.broadcasted_iota(jnp.int32, (SUB, DV), 0)
@@ -412,7 +475,7 @@
     fread[...] = jnp.broadcast_to(read, fread.shape)
 
     def copy_read(step):
-        target = base + (member + step) % heads
+        target = flip(step)
         return pltpu.make_async_remote_copy(
             src_ref=fread,
             dst_ref=rrecv.at[my_head],
@@ -427,9 +490,8 @@
     rrecv[my_head] = fread[...]
 
     for step in range(1, heads):
-        other = (member + heads - step) % heads
-        source = base + other
-        head = head_of(other)
+        source = flip(step)
+        head = head_of(source)
         pltpu.make_async_remote_copy(
             src_ref=fstate.at[source],
             dst_ref=srecv.at[head],
@@ -450,13 +512,11 @@
         state_out[h] = srecv[h]
         read_out[h : h + 1, :] = rrecv[h, 0:1, :]
 
-    for c in range(chunks):
-        copy_own(c).wait_send()
-        for step in range(1, n_y):
-            copy_peer(step, c).wait_send()
-            copy_forward(step, c).wait_send()
-    for step in range(1, n_sp):
-        copy_query(step).wait_send()
+    for k in range(parts):
+        copy_own(k).wait_send()
+        for step in range(1, n_y):
+            copy_peer(step, k).wait_send()
+            copy_forward(step, k).wait_send()
     for step in range(1, heads):
         copy_state(step).wait_send()
         copy_read(step).wait_send()
@@ -479,7 +539,7 @@
     tokens_here, features = tokens.shape
     depth, width = w_key.shape
     heads = width // DK
-    chunks = tokens_here // CHUNK
+    parts = tokens_here // CHUNK - 1 + tail_pieces(features)
     rows_out = DK // n_sp
     n_y = n_tp // 2
     levels = log2(n_sp)
@@ -488,12 +548,6 @@
     for _ in range(levels):
         count = max(count // 2, 1)
         slots += count
-    query = lax.dynamic_update_slice(
-        jnp.zeros((SUB, DK), F32),
-        new_query.astype(F32),
-        (0, lax.axis_index("sp") * rows_out),
-    )
-    increments = jnp.pad(forgetting_increment, ((0, SUB - heads), (0, 0)))
     vmem = pl.BlockSpec(memory_space=pltpu.VMEM)
     hbm = pl.BlockSpec(memory_space=pl.ANY)
     dma = pltpu.SemaphoreType.DMA
@@ -504,14 +558,17 @@
             jax.ShapeDtypeStruct((heads, rows_out, DV), BF16),
             jax.ShapeDtypeStruct((heads, DV), F32),
         ),
-        in_specs=[vmem, hbm, hbm, hbm, hbm, vmem, vmem, vmem, vmem, vmem],
+        in_specs=[hbm, hbm, hbm, hbm, hbm, vmem, vmem, vmem, vmem, vmem],
         out_specs=(vmem, vmem),
         scratch_shapes=[
             pltpu.VMEM((depth, width), BF16),
             pltpu.VMEM((depth, width), BF16),
-            pltpu.VMEM(w_beta.shape, BF16),
-            pltpu.VMEM(w_decay.shape, BF16),
+            pltpu.VMEM(w_beta.shape[::-1], BF16),
+            pltpu.VMEM(w_decay.shape[::-1], BF16),
             pltpu.VMEM((depth, LANES), BF16),
+            pltpu.VMEM((tokens_here, features), BF16),
+            pltpu.VMEM((SUB, tokens_here), F32),
+            pltpu.VMEM((SUB, DK), F32),
             pltpu.VMEM((n_tp, tokens_here, features), BF16),
             pltpu.VMEM((tokens_here, width), F32),
             pltpu.VMEM((tokens_here, width), F32),
@@ -527,13 +584,13 @@
             pltpu.VMEM((heads, rows_out, DV), BF16),
             pltpu.VMEM((SUB, DV), F32),
             pltpu.VMEM((heads, SUB, DV), F32),
-            dma((4,)),
-            dma((chunks,)),
-            dma((n_y, chunks)),
-            dma((n_y, chunks)),
-            dma((n_tp, chunks)),
-            dma((n_sp,)),
-            dma((n_sp,)),
+            dma((5,)),
+            dma((parts,)),
+            dma((n_y, parts)),
+            dma((n_y, parts)),
+            dma((n_tp, parts)),
+            dma((levels,)),
+            dma((levels,)),
             dma((levels,)),
             dma((levels,)),
             dma((levels,)),
@@ -550,12 +607,12 @@
         tokens,
         w_key,
         w_value,
-        w_beta,
-        w_decay,
+        w_beta.T,
+        w_decay.T,
         beta_bias[None, :],
         decay_rate[None, :],
-        increments,
-        query,
+        forgetting_increment,
+        new_query,
         read_gain[None, :],
     )
 

time: 63.1 us -> 57.3 us (0.908)
  local copies, waits for them, and re-layouts: 8.59 us -> 2.55 us
  Pallas kernels: 52.9 us -> 53.8 us
  other arithmetic: 0.68 us -> 0 us
    unnamed x6 -> x2, local copies, waits for them, and re-layouts: 7.07 us -> 2.55 us
    pad x1 -> x0, local copies, waits for them, and re-layouts: 1.31 us -> none  [per_device(): increments = jnp.pad(forgetting_increment, ((0, SUB - heads), (0, 0)))]
    pallas_call x1, Pallas kernels: 52.9 us -> 53.8 us  [per_device(): pl.pallas_call(functools.partial(body, n_sp, n_tp), name='delta_state', o...]
    convert_element_type x1 -> x0, other arithmetic: 0.68 us -> none  [per_device(): new_query.astype(F32)]
where the time goes in v2:
time: 57.3 us; the launch traced here: 57 us
  Pallas kernels  53.8 us (94%)
  local copies, waits for them, and re-layouts  2.55 us (4%)
  between operations  0.64 us (1%)
    pallas_call x1, Pallas kernels, per_device(): pl.pallas_call(functools.partial(body, n_sp, n_tp), name='delta_state', o...  53.8 us
    unnamed x2, local copies, waits for them, and re-layouts  2.55 us

profile of v2, /device:TPU:0, one launch (start us, length us, event | category | flops | bytes accessed | tf_op | source)
XLA Modules:
  0.0 57.0 jit_solution(16338307580551933936)
XLA Ops:
  0.6 53.8 %delta_state.1 = (bf16[4,16,128]{2,1,0:T(8,128)(2,1)}, f32[4,128]{1,0:T(4,128)}) custom-call(bf16[512,1024]{1,0:T(8,128)(2,1)} %x_hbm.1, bf16[4096,512]{1,0:T(8,128)(2,1)} %wk_hbm.1, bf16[4096,512]{1,0:T(8,128)(2,1)} %wv_hbm.1, bf16[16,4096]{1,0:T(8,128)(2,1)} %bitcast.5, bf16[16,4096]{1,0:T(8,128)(2,1)} %bitcast.6, f32[1,16]{1,0:T(1,128)} %bitcast.7, ...), custom_call_target="tpu_custom_call" | custom-call | tf_op jit(solution)/shard_map/delta_state/pallas_call | solution.py:554
  54.4 1.3 %copy.14 = bf16[4,16,128]{2,1,0:T(8,128)(2,1)} copy(bf16[4,16,128]{2,1,0:T(8,128)(2,1)} %get-tuple-element.4) | data formatting | bytes 32768
  55.8 1.2 %copy.15 = f32[4,128]{1,0:T(4,128)} copy(f32[4,128]{1,0:T(4,128)} %get-tuple-element.5) | data formatting | bytes 4096

commit v3 on v2

--- a/solution.py
+++ b/solution.py
@@ -522,6 +522,11 @@
         copy_read(step).wait_send()
 
 
+def hand_over(state_ref, read_ref, state_out, read_out):
+    state_out[...] = state_ref[...]
+    read_out[...] = read_ref[...]
+
+
 def per_device(
     n_sp,
     n_tp,
@@ -551,7 +556,7 @@
     vmem = pl.BlockSpec(memory_space=pltpu.VMEM)
     hbm = pl.BlockSpec(memory_space=pl.ANY)
     dma = pltpu.SemaphoreType.DMA
-    return pl.pallas_call(
+    state, read = pl.pallas_call(
         functools.partial(body, n_sp, n_tp),
         name="delta_state",
         out_shape=(
@@ -615,6 +620,16 @@
         new_query,
         read_gain[None, :],
     )
+    return pl.pallas_call(
+        hand_over,
+        name="hand_over",
+        out_shape=(
+            jax.ShapeDtypeStruct(state.shape, state.dtype),
+            jax.ShapeDtypeStruct(read.shape, read.dtype),
+        ),
+        in_specs=[vmem, vmem],
+        out_specs=(vmem, vmem),
+    )(state, read)
 
 
 def solution(mesh):

time: 57.3 us -> 56 us (0.977)
  local copies, waits for them, and re-layouts: 2.55 us -> 0 us
  Pallas kernels: 53.8 us -> 55.1 us
    unnamed x2 -> x0, local copies, waits for them, and re-layouts: 2.55 us -> none
    pallas_call x0 -> x1, Pallas kernels: none -> 1.33 us  [per_device(): pl.pallas_call(hand_over, name='hand_over', out_shape=(jax.ShapeDtypeStru...]
where the time goes in v3:
time: 56 us; the launch traced here: 55.8 us
  Pallas kernels  55.1 us (98%)
  between operations  0.64 us (1%)
    pallas_call x1, Pallas kernels, per_device(): pl.pallas_call(functools.partial(body, n_sp, n_tp), name='delta_state', o...  53.8 us
    pallas_call x1, Pallas kernels, per_device(): pl.pallas_call(hand_over, name='hand_over', out_shape=(jax.ShapeDtypeStru...  1.33 us

profile of v3, /device:TPU:0, one launch (start us, length us, event | category | flops | bytes accessed | tf_op | source)
XLA Modules:
  0.0 55.8 jit_solution(9779823972673796272)
XLA Ops:
  0.6 53.8 %delta_state.1 = (bf16[4,16,128]{2,1,0:T(8,128)(2,1)}, f32[4,128]{1,0:T(4,128)}) custom-call(bf16[512,1024]{1,0:T(8,128)(2,1)} %x_hbm.1, bf16[4096,512]{1,0:T(8,128)(2,1)} %wk_hbm.1, bf16[4096,512]{1,0:T(8,128)(2,1)} %wv_hbm.1, bf16[16,4096]{1,0:T(8,128)(2,1)} %bitcast.5, bf16[16,4096]{1,0:T(8,128)(2,1)} %bitcast.6, f32[1,16]{1,0:T(1,128)} %bitcast.7, ...), custom_call_target="tpu_custom_call" | custom-call | tf_op jit(solution)/shard_map/delta_state/pallas_call | solution.py:559
  54.4 1.3 %hand_over.1 = (bf16[4,16,128]{2,1,0:T(8,128)(2,1)}, f32[4,128]{1,0:T(4,128)}) custom-call(bf16[4,16,128]{2,1,0:T(8,128)(2,1)} %get-tuple-element.4.state_ref, f32[4,128]{1,0:T(4,128)} %get-tuple-element.5.read_ref), custom_call_target="tpu_custom_call" | custom-call | tf_op jit(solution)/shard_map/hand_over/pallas_call | solution.py:623
